TPU v7x, 32 devices: a whole 2x2x4 slice. The times are simulated.
32 devices in a mesh: sp: 8 (over z, x), tp: 4 (over y, core).
Axes of the slice: x: 2, y: 2, z: 4, core: 2. Of those that a mesh axis runs over, the one named last changes fastest.
Arguments:
- conv_value: bfloat16 [4096, 1024], P('sp', 'tp'), may hold values from -6 to 6
- conv_gate: bfloat16 [4096, 1024], P('sp', 'tp'), may hold values from -9 to 9
- conv_weight: float32 [31, 1024], P(None, 'tp'), may hold values from -2.2 to 2.2
- conv_gain: float32 [1024], P('tp'), may hold values from 0.1 to 1.9
- conv_shift: float32 [1024], P('tp'), may hold values from -3 to 3
- out_weight: bfloat16 [1024, 2048], P('tp'), may hold values from -0.1875 to 0.1875
- residual: bfloat16 [4096, 2048], P('sp', 'tp'), may hold values from -10 to 10
- mix_gain: float32 [2048], P('tp'), may hold values from 0.1 to 1.9
- expert_ids: int32 [4096, 2], P('sp'), may hold values from 0 to 7, all different within a row; in each aligned block of 128 rows (0 to 127, 128 to 255, ...) at most 64 rows name the same one
- group_weight: float32 [4096], P('sp'), may hold values from 0.6 to 1
- score_gap: float32 [4096], P('sp'), may hold values from -0.8 to 0.8
- w_gate: bfloat16 [8, 2048, 1024], P('sp', None, 'tp'), may hold values from -0.125 to 0.125
- w_up: bfloat16 [8, 2048, 1024], P('sp', None, 'tp'), may hold values from -0.125 to 0.125
- w_down: bfloat16 [8, 1024, 2048], P('sp', 'tp'), may hold values from -0.1875 to 0.1875
Outputs:
- layer_out: bfloat16 [4096, 2048], P('sp', 'tp')
Inputs may be any that keep to these rules, and one draw needn't show every extreme that they name: `expert_ids`: the two experts of a position differ. In each aligned block of 512 // 4 positions no expert is named by more than 64 rows, a bound that some block reaches.
All inputs are finite; a program needn't handle non-finite values.
Results may differ from a plain program's by a relative error of at most 0.012.
Values may be sent and summed in bfloat16 or wider, within the bound.
No kernel may reach another device: no remote copies, remote signals or barrier semaphores. Data moves between devices by JAX's collectives and lax.ppermute only.
A program may use at most 128 MiB of HBM per device.

v0:
```python
import jax
import jax.numpy as jnp
from jax import lax
from jax.sharding import PartitionSpec as P

D = 2048
CH = 1024


eps = 1e-06


def passed_along(value, axis, steps):
    count = lax.axis_size(axis)
    leading, last = (max(0, -steps), min(count, count - steps))
    return lax.ppermute(value, axis, [(source, source + steps) for source in range(leading, last)])


def shards(
    conv_value,
    conv_gate,
    conv_weight,
    conv_gain,
    conv_shift,
    out_weight,
    residual,
    mix_gain,
    expert_ids,
    group_weight,
    score_gap,
    w_gate,
    w_up,
    w_down,
):
    row_count = conv_value.shape[0]
    reach_rows = conv_weight.shape[0] - 1
    seq_devices = lax.axis_size("sp")
    tp_devices = lax.axis_size("tp")
    prev_value, prev_gate = passed_along(
        (conv_value[row_count - reach_rows :], conv_gate[row_count - reach_rows :]), "sp", 1
    )
    values = jnp.concatenate([prev_value, conv_value], axis=0).astype(jnp.float32)
    gate_pre = jnp.concatenate([prev_gate, conv_gate], axis=0).astype(jnp.float32)
    gated = values * jax.nn.sigmoid(gate_pre)
    convolved = jnp.zeros((row_count, conv_value.shape[1]), jnp.float32)
    for tap_index in range(reach_rows + 1):
        convolved = convolved + conv_weight[tap_index] * gated[tap_index : tap_index + row_count]
    row_sum, squares = lax.psum(
        (jnp.sum(convolved, axis=-1), jnp.sum(convolved * convolved, axis=-1)), "tp"
    )
    row_mean = (row_sum / CH)[:, None]
    row_var = (squares / CH)[:, None] - row_mean * row_mean
    normalized = (convolved - row_mean) * lax.rsqrt(row_var + eps) * conv_gain + conv_shift
    activated = jax.nn.silu(normalized).astype(jnp.bfloat16)
    partial_out = jnp.dot(activated, out_weight, preferred_element_type=jnp.float32)
    mixed = lax.psum_scatter(
        partial_out.astype(jnp.bfloat16), "tp", scatter_dimension=1, tiled=True
    ).astype(jnp.float32)
    middle = (residual.astype(jnp.float32) + mixed).astype(jnp.bfloat16)
    middle_wide = middle.astype(jnp.float32)
    row_sq = lax.psum(jnp.sum(middle_wide * middle_wide, axis=-1), "tp")
    normed = (middle_wide * lax.rsqrt(row_sq / D + eps)[:, None] * mix_gain).astype(jnp.bfloat16)
    quarter = row_count // tp_devices
    capacity = 4 * quarter // seq_devices
    expert_num = expert_ids.reshape(tp_devices, quarter * 2)
    onehot = (
        expert_num[:, :, None] == jnp.arange(seq_devices, dtype=jnp.int32)[None, None, :]
    ).astype(jnp.int32)
    before = jnp.cumsum(onehot, axis=1) - onehot
    ranking = jnp.sum(before * onehot, axis=-1)
    quarter_index = jnp.arange(tp_devices, dtype=jnp.int32)[:, None]
    slots = ((expert_num * tp_devices + quarter_index) * capacity + ranking).reshape(-1)
    own_rows = lax.all_to_all(normed, "tp", split_axis=0, concat_axis=1, tiled=True)
    my_index = lax.axis_index("tp")
    own_experts = lax.dynamic_slice_in_dim(expert_num, my_index, 1, 0)[0]
    own_rank = lax.dynamic_slice_in_dim(ranking, my_index, 1, 0)[0]
    own_slots = own_experts * capacity + own_rank
    token_of = jnp.arange(quarter * 2, dtype=jnp.int32) // 2
    outgoing = (
        jnp.zeros((seq_devices * capacity, D), jnp.bfloat16).at[own_slots].set(own_rows[token_of])
    )
    received = lax.all_to_all(
        outgoing.reshape(seq_devices, capacity, D), "sp", split_axis=0, concat_axis=0, tiled=True
    )
    gathered = lax.all_gather(received[:, None], "tp", axis=1, tiled=True)
    expert_in = gathered.reshape(-1, D)
    gate_part = jnp.dot(expert_in, w_gate[0], preferred_element_type=jnp.float32)
    up_part = jnp.dot(expert_in, w_up[0], preferred_element_type=jnp.float32)
    hidden = (jax.nn.silu(gate_part) * up_part).astype(jnp.bfloat16)
    partial_value = jnp.dot(hidden, w_down[0], preferred_element_type=jnp.float32)
    columns = lax.psum_scatter(
        partial_value.astype(jnp.bfloat16), "tp", scatter_dimension=1, tiled=True
    )
    col_count = columns.shape[1]
    returned = lax.all_to_all(
        columns.reshape(seq_devices, tp_devices * capacity, col_count),
        "sp",
        split_axis=0,
        concat_axis=0,
        tiled=True,
    )
    lookup = returned.reshape(-1, col_count)
    col_count = lookup.shape[1]
    picked = lookup[slots].reshape(row_count, 2, col_count).astype(jnp.float32)
    first_gate = group_weight * jax.nn.sigmoid(score_gap)
    second_gate = group_weight * jax.nn.sigmoid(-score_gap)
    result = middle_wide + first_gate[:, None] * picked[:, 0] + second_gate[:, None] * picked[:, 1]
    return result.astype(jnp.bfloat16)


def solution(mesh):
    return jax.shard_map(
        shards,
        mesh=mesh,
        in_specs=(
            P("sp", "tp"),
            P("sp", "tp"),
            P(None, "tp"),
            P("tp"),
            P("tp"),
            P("tp", None),
            P("sp", "tp"),
            P("tp"),
            P("sp", None),
            P("sp"),
            P("sp"),
            P("sp", None, "tp"),
            P("sp", None, "tp"),
            P("sp", "tp", None),
        ),
        out_specs=P("sp", "tp"),
        check_vma=False,
    )
```

profile of v0, /device:TPU:0, one launch (start us, length us, event | category | flops | bytes accessed | tf_op | source)
XLA Modules:
  0.0 363.9 jit_solution(2769100146873338767)
XLA Ops:
  6.5 0.8 slice.205
  7.4 4.9 %collective-permute-start = (bf16[30,256]{1,0:T(8,128)(2,1)S(1)}, bf16[30,256]{1,0:T(8,128)(2,1)S(1)}, u32[]{:S(2)}, u32[]{:S(2)}) collective-permute-start(bf16[30,256]{1,0:T(8,128)(2,1)S(1)} %slice.205), channel_id=1, source_target_pairs={{0,4},{4,8},{8,12},{12,16},{16,20},{20,24},{24,28},{1,5},{5,9},{9,... | collective-permute-start | bytes 46088 | tf_op jit(solution)/shard_map/ppermute | solution.py:16
  12.2 0.7 slice.206
  12.9 3.4 collective-permute-start.1
  16.4 1.0 fusion.62
  17.4 1.0 fusion.63
  18.4 1.2 divide_multiply_fusion
  19.7 0.0 copy-start.8
  19.7 0.0 copy-start.11
  19.7 0.0 copy-start.12
  19.7 2.4 fusion.59
  22.1 6.1 %all-reduce = (f32[512]{0:T(512)S(1)}, f32[512]{0:T(512)S(1)}) all-reduce(f32[512]{0:T(512)S(1)} %get-tuple-element.6, f32[512]{0:T(512)S(1)} %get-tuple-element.5), channel_id=1, replica_groups=mesh['sp'=8,'tp'=4] {'tp'}, use_global_device_ids=true, to_apply=%region_3.0 | all-reduce | flops 1024 | bytes 8192 | tf_op jit(solution)/shard_map/psum | solution.py:48
  28.2 2.1 convolution_convert_fusion.1
  30.3 0.0 reduce-scatter.3.cloned.1.call-update
  30.3 0.7 copy-done.4
  31.0 0.1 copy.18
  31.2 0.2 eq.26
  31.3 2.3 reduce-window.6
  33.6 0.1 slice.307
  33.7 0.1 copy.20
  33.8 29.0 %reduce-scatter.3.cloned.1.call-done = bf16[512,512]{1,0:T(8,128)(2,1)} async-done(((bf16[512,2048]{1,0:T(8,128)(2,1)}), bf16[512,512]{1,0:T(8,128)(2,1)}) %reduce-scatter.3.cloned.1.call-update) | async-done | bytes 524304 | tf_op jit(solution)/shard_map/reduce_scatter | solution.py:56
  62.9 1.3 fusion.1
  64.1 5.8 %psum.23 = f32[512]{0:T(512)S(1)} all-reduce(f32[512]{0:T(512)S(1)} %fusion.1), channel_id=1, replica_groups=mesh['sp'=8,'tp'=4] {'tp'}, use_global_device_ids=true, to_apply=%region_9.10 | all-reduce | flops 512 | bytes 4096 | tf_op jit(solution)/shard_map/psum | solution.py:61
  69.9 2.0 fusion.3
  72.0 3.5 all-to-all-start
  75.4 0.0 all-gather.3.cloned.1.call-start
  75.5 0.2 reshape.168
  75.7 0.1 fusion.53
  75.8 8.4 %all-to-all-done = bf16[4,128,512]{2,1,0:T(8,128)(2,1)S(1)} async-done(((bf16[4,128,512]{2,1,0:T(8,128)(2,1)}), bf16[4,128,512]{2,1,0:T(8,128)(2,1)S(1)}, u32[]{:S(2)}, u32[]{:S(2)}) %all-to-all-start) | async-done | bytes 524320 | tf_op jit(solution)/shard_map/all_to_all | solution.py:73
  84.2 0.9 copy.28
  85.1 6.4 %scatter_custom_fusion = bf16[512,2048]{1,0:T(8,128)(2,1)S(1)} fusion(s32[256]{0:T(256)S(1)} %bitcast.130, bf16[128,2048]{1,0:T(8,128)(2,1)} %bitcast.93, s32[1024]{0:T(1024)S(1)} %pad_clamp_fusion, bf16[]{:T(256)} %constant.25.clone.1), kind=kCustom, calls=%fused_computation.23 | custom fusion | bytes 2097664 | tf_op jit(solution)/shard_map/scatter | solution.py:80
  91.4 53.6 %all_to_all.29 = bf16[8,64,2048]{2,1,0:T(8,128)(2,1)} all-to-all(bf16[8,64,2048]{2,1,0:T(8,128)(2,1)S(1)} %bitcast.90), channel_id=1, replica_groups=mesh['sp'=8,'tp'=4] {'sp'}, dimensions={0} | all-to-all | bytes 4194304 | tf_op jit(solution)/shard_map/all_to_all | solution.py:82
  145.1 0.0 all-gather.3.cloned.1.call-update
  145.1 0.2 reduce-scatter.5.cloned.1.call-start
  145.3 56.4 %all-gather.3.cloned.1.call-done = bf16[8,256,2048]{2,1,0:T(8,128)(2,1)} async-done(((bf16[8,64,2048]{2,1,0:T(8,128)(2,1)}), bf16[8,256,2048]{2,1,0:T(8,128)(2,1)}) %all-gather.3.cloned.1.call-update) | async-done | bytes 8388624 | tf_op jit(solution)/shard_map/all_gather | solution.py:85
  201.7 7.2 %fusion.11 = f32[2048,256]{1,0:T(8,128)} fusion(bf16[2048,2048]{1,0:T(8,128)(2,1)} %bitcast.131, bf16[1,2048,256]{2,1,0:T(8,128)(2,1)S(1)} %copy-done.9), kind=kOutput, calls=%fused_computation.21 | convolution fusion | flops 2147483648 | bytes 11534336 | tf_op jit(solution)/shard_map/dot_general | solution.py:87
  208.9 13.1 %convolution_convert_fusion = bf16[2048,2048]{1,0:T(8,128)(2,1)} fusion(bf16[2048,2048]{1,0:T(8,128)(2,1)} %bitcast.132, f32[2048,256]{1,0:T(8,128)} %fusion.11, bf16[1,256,2048]{2,1,0:T(8,128)(2,1)S(1)} %copy-done, bf16[1,2048,256]{2,1,0:T(8,128)(2,1)S(1)} %copy-done.10), kind=kOutput, calls=%fused_computation.3 | convolution fusion | flops 4302307328 | bytes 20971520 | tf_op jit(solution)/shard_map/dot_general | solution.py:90
  222.0 0.0 reduce-scatter.5.cloned.1.call-update
  222.0 71.4 %reduce-scatter.5.cloned.1.call-done = bf16[2048,512]{1,0:T(8,128)(2,1)} async-done(((bf16[2048,2048]{1,0:T(8,128)(2,1)}), bf16[2048,512]{1,0:T(8,128)(2,1)}) %reduce-scatter.5.cloned.1.call-update) | async-done | bytes 2097168 | tf_op jit(solution)/shard_map/reduce_scatter | solution.py:91
  293.4 5.6 %all-to-all-start.2 = ((bf16[8,256,512]{2,1,0:T(8,128)(2,1)}), bf16[8,256,512]{2,1,0:T(8,128)(2,1)S(1)}, u32[]{:S(2)}, u32[]{:S(2)}) async-start(bf16[8,256,512]{2,1,0:T(8,128)(2,1)} %bitcast.91), calls=%async_computation.4 | async-start | bytes 4194304 | tf_op jit(solution)/shard_map/all_to_all | solution.py:95
  299.1 0.1 copy.23
  299.2 0.2 mul.551
  299.5 47.6 %all-to-all-done.2 = bf16[8,256,512]{2,1,0:T(8,128)(2,1)S(1)} async-done(((bf16[8,256,512]{2,1,0:T(8,128)(2,1)}), bf16[8,256,512]{2,1,0:T(8,128)(2,1)S(1)}, u32[]{:S(2)}, u32[]{:S(2)}) %all-to-all-start.2) | async-done | bytes 2097184 | tf_op jit(solution)/shard_map/all_to_all | solution.py:95
  347.2 5.0 %gather_fusion = bf16[1024,512]{1,0:T(8,128)(2,1)} fusion(bf16[2048,512]{1,0:T(8,128)(2,1)S(1)} %bitcast.89, s32[1024]{0:T(1024)S(1)} %broadcast_clamp_fusion), kind=kCustom, calls=%fused_computation.1 | custom fusion | bytes 2101248 | tf_op jit(solution)/shard_map/gather | solution.py:104
  352.2 2.4 reshape.174
  354.6 0.0 copy-start.2
  354.6 1.6 fusion.61
  356.3 1.1 fusion.5
  (40 shorter events, 0.2 us)
Async XLA Ops:
  6.5 202.4 %copy-start = (bf16[1,256,2048]{2,1,0:T(8,128)(2,1)S(1)}, bf16[1,256,2048]{2,1,0:T(8,128)(2,1)}, u32[]{:S(2)}) copy-start(bf16[1,256,2048]{2,1,0:T(8,128)(2,1)} %param.27) | copy-start | bytes 3145732
  6.5 56.3 %reduce-scatter.3.cloned.1.call-start = ((), (), s32[]{:S(2)}) async-start(), calls=%async_computation.5 | async-start | bytes 2621440 | tf_op jit(solution)/shard_map/reduce_scatter | solution.py:56
  7.4 11.1 %collective-permute-start = (bf16[30,256]{1,0:T(8,128)(2,1)S(1)}, bf16[30,256]{1,0:T(8,128)(2,1)S(1)}, u32[]{:S(2)}, u32[]{:S(2)}) collective-permute-start(bf16[30,256]{1,0:T(8,128)(2,1)S(1)} %slice.205), channel_id=1, source_target_pairs={{0,4},{4,8},{8,12},{12,16},{16,20},{20,24},{24,28},{1,5},{5,9},{9,... | collective-permute-start | bytes 46088 | tf_op jit(solution)/shard_map/ppermute | solution.py:16
  12.9 5.5 %collective-permute-start.1 = (bf16[30,256]{1,0:T(8,128)(2,1)S(1)}, bf16[30,256]{1,0:T(8,128)(2,1)S(1)}, u32[]{:S(2)}, u32[]{:S(2)}) collective-permute-start(bf16[30,256]{1,0:T(8,128)(2,1)S(1)} %slice.206), channel_id=1, source_target_pairs={{0,4},{4,8},{8,12},{12,16},{16,20},{20,24},{24,28},{1,5},{5,9},{9,... | collective-permute-start | bytes 46088 | tf_op jit(solution)/shard_map/ppermute | solution.py:16
  19.7 8.5 %copy-start.8 = (bf16[256,2048]{1,0:T(8,128)(2,1)S(1)}, bf16[256,2048]{1,0:T(8,128)(2,1)}, u32[]{:S(2)}) copy-start(bf16[256,2048]{1,0:T(8,128)(2,1)} %param.19) | copy-start | bytes 3145732
  19.7 8.5 %copy-start.11 = (f32[256]{0:T(256)S(1)}, f32[256]{0:T(256)}, u32[]{:S(2)}) copy-start(f32[256]{0:T(256)} %param.18) | copy-start | bytes 3076
  19.7 8.5 %copy-start.12 = (f32[256]{0:T(256)S(1)}, f32[256]{0:T(256)}, u32[]{:S(2)}) copy-start(f32[256]{0:T(256)} %param.17) | copy-start | bytes 3076
  30.3 0.7 copy-start.4
  30.3 32.5 %copy-start.1 = (bf16[512,512]{1,0:T(8,128)(2,1)S(1)}, bf16[512,512]{1,0:T(8,128)(2,1)}, u32[]{:S(2)}) copy-start(bf16[512,512]{1,0:T(8,128)(2,1)} %param.20) | copy-start | bytes 1572868
  30.3 39.6 %copy-start.5 = (f32[512]{0:T(512)S(1)}, f32[512]{0:T(512)}, u32[]{:S(2)}) copy-start(f32[512]{0:T(512)} %param.21) | copy-start | bytes 6148
  72.0 12.3 %all-to-all-start = ((bf16[4,128,512]{2,1,0:T(8,128)(2,1)}), bf16[4,128,512]{2,1,0:T(8,128)(2,1)S(1)}, u32[]{:S(2)}, u32[]{:S(2)}) async-start(bf16[4,128,512]{2,1,0:T(8,128)(2,1)} %bitcast.36), calls=%async_computation.1 | async-start | bytes 1048576 | tf_op jit(solution)/shard_map/all_to_all | solution.py:73
  75.4 126.3 %all-gather.3.cloned.1.call-start = ((), (), s32[]{:S(2)}) async-start(), calls=%async_computation.7 | async-start | bytes 10485760 | tf_op jit(solution)/shard_map/all_gather | solution.py:85
  145.1 56.7 %copy-start.9 = (bf16[1,2048,256]{2,1,0:T(8,128)(2,1)S(1)}, bf16[1,2048,256]{2,1,0:T(8,128)(2,1)}, u32[]{:S(2)}) copy-start(bf16[1,2048,256]{2,1,0:T(8,128)(2,1)} %param.25) | copy-start | bytes 3145732
  145.1 148.3 %reduce-scatter.5.cloned.1.call-start = ((), (), s32[]{:S(2)}) async-start(), calls=%async_computation.6 | async-start | bytes 10485760 | tf_op jit(solution)/shard_map/reduce_scatter | solution.py:91
  201.7 7.2 %copy-start.10 = (bf16[1,2048,256]{2,1,0:T(8,128)(2,1)S(1)}, bf16[1,2048,256]{2,1,0:T(8,128)(2,1)}, u32[]{:S(2)}) copy-start(bf16[1,2048,256]{2,1,0:T(8,128)(2,1)} %param.26) | copy-start | bytes 3145732
  293.4 6.1 %copy-start.6 = (f32[512]{0:T(512)S(1)}, f32[512]{0:T(512)}, u32[]{:S(2)}) copy-start(f32[512]{0:T(512)} %param.23) | copy-start | bytes 6148
  293.4 6.1 %copy-start.7 = (f32[512]{0:T(512)S(1)}, f32[512]{0:T(512)}, u32[]{:S(2)}) copy-start(f32[512]{0:T(512)} %param.24) | copy-start | bytes 6148
  293.4 53.7 %all-to-all-start.2 = ((bf16[8,256,512]{2,1,0:T(8,128)(2,1)}), bf16[8,256,512]{2,1,0:T(8,128)(2,1)S(1)}, u32[]{:S(2)}, u32[]{:S(2)}) async-start(bf16[8,256,512]{2,1,0:T(8,128)(2,1)} %bitcast.91), calls=%async_computation.4 | async-start | bytes 4194304 | tf_op jit(solution)/shard_map/all_to_all | solution.py:95
  354.6 1.7 copy-start.2
  354.6 1.6 copy-start.3
Sparse Core Ops, SparseCore 0:
  30.5 32.3 reduce-scatter.2
  145.2 56.4 all-gather.2
  222.2 71.2 reduce-scatter.4
where the time goes:
time: 365 us; the launch traced here: 364 us
  waiting for transfers between devices  213 us (58%)
  blocking collectives  65.4 us (18%)
  matrix products  22.4 us (6%)
  local copies, waits for them, and re-layouts  21.5 us (6%)
  starting transfers between devices  17.7 us (5%)
  between operations  13.4 us (4%)
  other arithmetic  10.5 us (3%)
    reduce_scatter x1, waiting for transfers between devices, shards(): lax.psum_scatter(partial_value.astype(jnp.bfloat16), 'tp', scatter_dimens...  71.4 us
    all_gather x1, waiting for transfers between devices, shards(): gathered = lax.all_gather(received[:, None], 'tp', axis=1, tiled=True)  56.4 us
    all_to_all x1, blocking collectives, shards(): lax.all_to_all(outgoing.reshape(seq_devices, capacity, D), 'sp', split_ax...  53.6 us
    all_to_all x1, waiting for transfers between devices, shards(): lax.all_to_all(columns.reshape(seq_devices, tp_devices * capacity, col_co...  47.6 us
    reduce_scatter x1, waiting for transfers between devices, shards(): lax.psum_scatter(partial_out.astype(jnp.bfloat16), 'tp', scatter_dimensio...  29 us
    dot_general x1, matrix products, shards(): jnp.dot(hidden, w_down[0], preferred_element_type=jnp.float32)  13.1 us
    all_to_all x1, waiting for transfers between devices, shards(): lax.all_to_all(normed, 'tp', split_axis=0, concat_axis=1, tiled=True)  8.4 us
    ppermute x2, starting transfers between devices, passed_along(): lax.ppermute(value, axis, [(source, source + steps) for source in range(l...  8.3 us
  transfers between devices with their start and end apart: 7, of which 5 were waited for; matrix products, arithmetic and copies ran while one was open for 2% of the time, Pallas kernels for 0%

commit v1 on v0

v1 whole, which is shorter than its diff:
```python
import jax
import jax.numpy as jnp
from jax import lax
from jax.sharding import PartitionSpec as P


D = 2048
CH = 1024


eps = 1e-06


def swap(value, bit):
    count = lax.axis_size("tp")
    return lax.ppermute(value, "tp", [(source, source ^ bit) for source in range(count)])


def natural(blocks, index):
    ordered = []
    for place in range(len(blocks)):
        chosen = blocks[0]
        for bit in range(1, len(blocks)):
            chosen = jnp.where(index == (place ^ bit), blocks[bit], chosen)
        ordered.append(chosen)
    return ordered


def exchanged(piece):
    count = lax.axis_size("tp")
    blocks = [piece(0)]
    for bit in range(1, count):
        blocks.append(swap(piece(bit), bit))
    return blocks


def gathered(block):
    count = lax.axis_size("tp")
    held = {0: block}
    bit = count // 2
    while bit:
        for have in sorted(held):
            held[bit ^ have] = swap(held[have], bit)
        bit //= 2
    return [held[bit] for bit in range(count)]


def dot(left, right):
    return jnp.dot(left, right, preferred_element_type=jnp.float32)


def shards(
    conv_value,
    conv_gate,
    conv_weight,
    conv_gain,
    conv_shift,
    out_weight,
    residual,
    mix_gain,
    expert_ids,
    group_weight,
    score_gap,
    w_gate,
    w_up,
    w_down,
):
    row_count, width = conv_value.shape
    taps = conv_weight.shape[0]
    reach = taps - 1
    halo = -(-reach // 16) * 16
    seq_devices = lax.axis_size("sp")
    tp_devices = lax.axis_size("tp")
    quarter = row_count // tp_devices
    capacity = 4 * quarter // seq_devices
    slots = seq_devices * capacity
    col_count = residual.shape[1]
    tp = lax.axis_index("tp")

    gated = conv_value.astype(jnp.float32) * jax.nn.sigmoid(conv_gate.astype(jnp.float32))
    gated = gated.astype(jnp.bfloat16)
    previous = lax.ppermute(
        gated[row_count - halo :], "sp", [(i, i + 1) for i in range(seq_devices - 1)]
    )
    padded = jnp.concatenate([previous, gated], axis=0)
    windows = exchanged(
        lambda bit: lax.dynamic_slice_in_dim(padded, (tp ^ bit) * quarter, halo + quarter, 0),
    )
    small = jnp.concatenate(
        [conv_weight, conv_gain[None], conv_shift[None], mix_gain.reshape(-1, width)], axis=0
    )
    smalls = exchanged(lambda bit: small)

    out_weights = gathered(out_weight)
    residuals = natural(
        exchanged(lambda bit: lax.dynamic_slice_in_dim(residual, (tp ^ bit) * quarter, quarter, 0)),
        tp,
    )
    gates = gathered(w_gate[0])
    ups = gathered(w_up[0])
    downs = gathered(w_down[0])

    ids = lax.dynamic_slice_in_dim(expert_ids, tp * quarter, quarter, 0)
    experts = jnp.arange(seq_devices, dtype=jnp.int32)[None]
    first_hot = (ids[:, :1] == experts).astype(jnp.bfloat16)
    second_hot = (ids[:, 1:] == experts).astype(jnp.bfloat16)
    earlier = jnp.tri(quarter, k=-1, dtype=jnp.bfloat16)
    before = dot(earlier, first_hot + second_hot)
    slot_ids = jnp.arange(slots, dtype=jnp.int32)[None]
    first_rank = jnp.sum(before * first_hot, axis=1).astype(jnp.int32)
    second_rank = jnp.sum(before * second_hot, axis=1).astype(jnp.int32)
    first_pick = ((ids[:, 0] * capacity + first_rank)[:, None] == slot_ids).astype(jnp.bfloat16)
    second_pick = ((ids[:, 1] * capacity + second_rank)[:, None] == slot_ids).astype(jnp.bfloat16)
    weights = lax.dynamic_slice_in_dim(group_weight, tp * quarter, quarter, 0)
    gaps = lax.dynamic_slice_in_dim(score_gap, tp * quarter, quarter, 0)
    first_gate = (weights * jax.nn.sigmoid(gaps))[:, None]
    second_gate = (weights * jax.nn.sigmoid(-gaps))[:, None]

    convolved = []
    for window, part in zip(windows, smalls):
        wide = window.astype(jnp.float32)
        total = jnp.zeros((quarter, width), jnp.float32)
        for tap in range(taps):
            start = halo - reach + tap
            total = total + part[tap] * wide[start : start + quarter]
        convolved.append(total)
    row_mean = sum(jnp.sum(c, axis=-1, keepdims=True) for c in convolved) / CH
    row_var = sum(jnp.sum(c * c, axis=-1, keepdims=True) for c in convolved) / CH
    row_var = row_var - row_mean * row_mean
    scale = lax.rsqrt(row_var + eps)
    mixed = 0.0
    for c, part, weight in zip(convolved, smalls, out_weights):
        normalized = (c - row_mean) * scale * part[taps] + part[taps + 1]
        mixed = mixed + dot(jax.nn.silu(normalized).astype(jnp.bfloat16), weight)
    middle = (jnp.concatenate(residuals, axis=1).astype(jnp.float32) + mixed).astype(jnp.bfloat16)
    middle_wide = middle.astype(jnp.float32)
    row_sq = jnp.sum(middle_wide * middle_wide, axis=-1, keepdims=True)
    gain = jnp.concatenate([g[taps + 2 :].reshape(-1) for g in natural(smalls, tp)])
    normed = (middle_wide * lax.rsqrt(row_sq / D + eps) * gain).astype(jnp.bfloat16)

    outgoing = lax.dot_general(
        first_pick + second_pick,
        normed,
        (((0,), (0,)), ((), ())),
        preferred_element_type=jnp.float32,
    ).astype(jnp.bfloat16)
    received = lax.all_to_all(
        outgoing.reshape(seq_devices, capacity, D), "sp", 0, 0, tiled=True
    ).reshape(slots, D)
    total = 0.0
    for gate, up, down in zip(gates, ups, downs):
        hidden = (jax.nn.silu(dot(received, gate)) * dot(received, up)).astype(jnp.bfloat16)
        total = total + dot(hidden, down)
    returned = lax.all_to_all(
        total.astype(jnp.bfloat16).reshape(seq_devices, capacity, D), "sp", 0, 0, tiled=True
    ).reshape(slots, D)

    picked = first_gate * dot(first_pick, returned) + second_gate * dot(second_pick, returned)
    result = (middle_wide + picked).astype(jnp.bfloat16)
    rows = natural(
        exchanged(
            lambda bit: lax.dynamic_slice_in_dim(result, (tp ^ bit) * col_count, col_count, 1),
        ),
        tp,
    )
    return jnp.concatenate(rows, axis=0)


def solution(mesh):
    return jax.shard_map(
        shards,
        mesh=mesh,
        in_specs=(
            P("sp", "tp"),
            P("sp", "tp"),
            P(None, "tp"),
            P("tp"),
            P("tp"),
            P("tp", None),
            P("sp", "tp"),
            P("tp"),
            P("sp", None),
            P("sp"),
            P("sp"),
            P("sp", None, "tp"),
            P("sp", None, "tp"),
            P("sp", "tp", None),
        ),
        out_specs=P("sp", "tp"),
        check_vma=False,
    )
```

time: 365 us -> 224 us (0.61)
  waiting for transfers between devices: 213 us -> 138 us
  blocking collectives: 65.4 us -> 0 us
  matrix products: 22.4 us -> 43.2 us
  local copies, waits for them, and re-layouts: 21.5 us -> 4.85 us
  between operations: 13.4 us -> 0.45 us
  starting transfers between devices: 17.7 us -> 28.5 us
    reduce_scatter x2 -> x0, waiting for transfers between devices: 100 us -> none  [the longest x1 71.4 us: shards(): lax.psum_scatter(partial_value.astype(jnp.bfloat16), 'tp', scatter_dimens...]
    ppermute x2 -> x25, waiting for transfers between devices: 0.01 us -> 67.4 us  [the longest x24 67.4 us: swap(): lax.ppermute(value, 'tp', [(source, source ^ bit) for source in range(cou...]
    all_gather x1 -> x0, waiting for transfers between devices: 56.4 us -> none  [shards(): gathered = lax.all_gather(received[:, None], 'tp', axis=1, tiled=True)]
    all_to_all x1 -> x0, blocking collectives: 53.6 us -> none  [shards(): lax.all_to_all(outgoing.reshape(seq_devices, capacity, D), 'sp', split_ax...]
    dot_general x3 -> x16, matrix products: 22.4 us -> 43.2 us  [the longest x15 41 us: dot(): return jnp.dot(left, right, preferred_element_type=jnp.float32)]
    all_to_all x2, waiting for transfers between devices: 56 us -> 70.6 us  [the longest x1 48.1 us: shards(): lax.all_to_all(total.astype(jnp.bfloat16).reshape(seq_devices, capacity,...]
    psum x2 -> x0, blocking collectives: 11.8 us -> none  [the longest x1 6.05 us: shards(): lax.psum((jnp.sum(convolved, axis=-1), jnp.sum(convolved * convolved, axi...]
    ppermute x2 -> x25, starting transfers between devices: 8.3 us -> 17.9 us  [the longest x24 14.3 us: swap(): lax.ppermute(value, 'tp', [(source, source ^ bit) for source in range(cou...]
  transfers between devices with their start and end apart: 7 -> 27, of which waited for: 5 -> 8; matrix products, arithmetic and copies ran while one was open for 2% -> 17% of each run, Pallas kernels for 0% -> 0%
where the time goes in v1:
time: 224 us; the launch traced here: 223 us
  waiting for transfers between devices  138 us (62%)
  matrix products  43.2 us (19%)
  starting transfers between devices  28.5 us (13%)
  other arithmetic  8.23 us (4%)
  local copies, waits for them, and re-layouts  4.85 us (2%)
    ppermute x24, waiting for transfers between devices, swap(): lax.ppermute(value, 'tp', [(source, source ^ bit) for source in range(cou...  67.4 us
    all_to_all x1, waiting for transfers between devices, shards(): lax.all_to_all(total.astype(jnp.bfloat16).reshape(seq_devices, capacity,...  48.1 us
    dot_general x15, matrix products, dot(): return jnp.dot(left, right, preferred_element_type=jnp.float32)  41 us
    all_to_all x1, waiting for transfers between devices, shards(): lax.all_to_all(outgoing.reshape(seq_devices, capacity, D), 'sp', 0, 0, ti...  22.5 us
    ppermute x24, starting transfers between devices, swap(): lax.ppermute(value, 'tp', [(source, source ^ bit) for source in range(cou...  14.3 us
    all_to_all x1, starting transfers between devices, shards(): lax.all_to_all(total.astype(jnp.bfloat16).reshape(seq_devices, capacity,...  5.72 us
    all_to_all x1, starting transfers between devices, shards(): lax.all_to_all(outgoing.reshape(seq_devices, capacity, D), 'sp', 0, 0, ti...  4.88 us
  transfers between devices with their start and end apart: 27, of which 8 were waited for; matrix products, arithmetic and copies ran while one was open for 17% of the time, Pallas kernels for 0%

profile of v1, /device:TPU:0, one launch (start us, length us, event | category | flops | bytes accessed | tf_op | source)
XLA Modules:
  0.0 223.2 jit_solution(4383282466194923630)
XLA Ops:
  0.0 0.7 reshape.104
  0.7 0.8 pad_maximum_fusion.1
  1.5 0.6 collective-permute-start.4
  2.1 2.6 %collective-permute-start.6 = (f32[35,256]{1,0:T(8,128)S(1)}, f32[35,256]{1,0:T(8,128)S(1)}, u32[]{:S(2)}, u32[]{:S(2)}) collective-permute-start(f32[35,256]{1,0:T(8,128)S(1)} %pad_maximum_fusion.1), channel_id=1, source_target_pairs={{0,2},{1,3},{2,0},{3,1},{4,6},{5,7},{6,4},{7,5},{8,10},{9,11},{10,... | collective-permute-start | bytes 107528 | tf_op jit(solution)/shard_map/ppermute | solution.py:16
  4.7 1.2 multiply_convert_fusion.5
  5.9 3.6 %collective-permute-start.3 = (bf16[32,256]{1,0:T(8,128)(2,1)S(1)}, bf16[32,256]{1,0:T(8,128)(2,1)S(1)}, u32[]{:S(2)}, u32[]{:S(2)}) collective-permute-start(bf16[32,256]{1,0:T(8,128)(2,1)S(1)} %slice.1046), channel_id=1, source_target_pairs={{0,4},{4,8},{8,12},{12,16},{16,20},{20,24},{24,28},{1,5},{5,9},{9,... | collective-permute-start | bytes 49160 | tf_op jit(solution)/shard_map/ppermute | solution.py:82
  9.7 1.0 fusion.209
  10.7 1.0 fusion.210
  12.0 1.1 constant_dynamic-slice_fusion.4
  13.1 1.6 collective-permute-start.11
  14.8 0.6 multiply_reduce_fusion.4
  16.1 1.5 collective-permute-start.7
  17.9 0.7 collective-permute-start.1
  18.5 25.4 %collective-permute-done.7 = bf16[160,256]{1,0:T(8,128)(2,1)S(1)} collective-permute-done((bf16[160,256]{1,0:T(8,128)(2,1)S(1)}, bf16[160,256]{1,0:T(8,128)(2,1)S(1)}, u32[]{:S(2)}, u32[]{:S(2)}) %collective-permute-start.7) | collective-permute-done | bytes 81952 | tf_op jit(solution)/shard_map/ppermute | solution.py:16
  44.2 0.6 multiply_reduce_fusion.3
  44.7 0.6 multiply_reduce_fusion.2
  45.3 3.4 %collective-permute-done.9 = bf16[160,256]{1,0:T(8,128)(2,1)S(1)} collective-permute-done((bf16[160,256]{1,0:T(8,128)(2,1)S(1)}, bf16[160,256]{1,0:T(8,128)(2,1)S(1)}, u32[]{:S(2)}, u32[]{:S(2)}) %collective-permute-start.9) | collective-permute-done | bytes 81952 | tf_op jit(solution)/shard_map/ppermute | solution.py:16
  48.8 0.6 multiply_reduce_fusion.1
  50.4 1.1 select_select_fusion.7
  52.3 0.5 multiply_reduce_fusion
  52.8 2.2 convolution_convert_fusion
  55.0 4.9 %all-to-all-start = ((bf16[8,64,2048]{2,1,0:T(8,128)(2,1)}), bf16[8,64,2048]{2,1,0:T(8,128)(2,1)S(1)}, u32[]{:S(2)}, u32[]{:S(2)}) async-start(bf16[8,64,2048]{2,1,0:T(8,128)(2,1)} %bitcast.208), calls=%async_computation | async-start | bytes 4194304 | tf_op jit(solution)/shard_map/all_to_all | solution.py:147
  59.9 0.8 collective-permute-start.16
  60.7 0.5 collective-permute-start.14
  61.2 1.2 collective-permute-start.17
  62.4 0.8 collective-permute-start.18
  63.2 23.0 %collective-permute-done.16 = bf16[2048,256]{1,0:T(8,128)(2,1)} collective-permute-done((bf16[2048,256]{1,0:T(8,128)(2,1)}, bf16[2048,256]{1,0:T(8,128)(2,1)}, u32[]{:S(2)}, u32[]{:S(2)}) %collective-permute-start.16) | collective-permute-done | bytes 1048608 | tf_op jit(solution)/shard_map/ppermute | solution.py:16
  86.2 22.5 %all-to-all-done = bf16[8,64,2048]{2,1,0:T(8,128)(2,1)S(1)} async-done(((bf16[8,64,2048]{2,1,0:T(8,128)(2,1)}), bf16[8,64,2048]{2,1,0:T(8,128)(2,1)S(1)}, u32[]{:S(2)}, u32[]{:S(2)}) %all-to-all-start) | async-done | bytes 2097184 | tf_op jit(solution)/shard_map/all_to_all | solution.py:147
  108.7 2.7 %fusion.189 = f32[512,256]{1,0:T(8,128)} fusion(bf16[512,2048]{1,0:T(8,128)(2,1)S(1)} %bitcast.197, bf16[1,2048,256]{2,1,0:T(8,128)(2,1)} %param.25), kind=kOutput, calls=%fused_computation.378 | convolution fusion | flops 536870912 | bytes 3670016 | tf_op jit(solution)/shard_map/dot_general | solution.py:49
  111.4 2.7 %fusion.218 = f32[512,256]{1,0:T(8,128)} fusion(bf16[512,2048]{1,0:T(8,128)(2,1)S(1)} %bitcast.198, bf16[2048,256]{1,0:T(8,128)(2,1)} %collective-permute-done.16), kind=kOutput, calls=%fused_computation.400 | convolution fusion | flops 536870912 | bytes 3670016 | tf_op jit(solution)/shard_map/dot_general | solution.py:49
  114.2 6.0 %fusion.7 = f32[512,2048]{1,0:T(8,128)} fusion(bf16[512,2048]{1,0:T(8,128)(2,1)S(1)} %bitcast.199, f32[512,256]{1,0:T(8,128)} %fusion.189, bf16[1,256,2048]{2,1,0:T(8,128)(2,1)} %param.27, bf16[1,2048,256]{2,1,0:T(8,128)(2,1)} %param.26), kind=kOutput, calls=%fused_computation.15 | convolution fusion | flops 1074528256 | bytes 8912896 | tf_op jit(solution)/shard_map/dot_general | solution.py:49
  120.6 9.7 %collective-permute-done.18 = bf16[256,2048]{1,0:T(8,128)(2,1)} collective-permute-done((bf16[256,2048]{1,0:T(8,128)(2,1)}, bf16[256,2048]{1,0:T(8,128)(2,1)}, u32[]{:S(2)}, u32[]{:S(2)}) %collective-permute-start.18) | collective-permute-done | bytes 1048608 | tf_op jit(solution)/shard_map/ppermute | solution.py:16
  130.3 2.7 %fusion.217 = f32[512,256]{1,0:T(8,128)} fusion(bf16[512,2048]{1,0:T(8,128)(2,1)S(1)} %bitcast.200, bf16[2048,256]{1,0:T(8,128)(2,1)} %collective-permute-done.13), kind=kOutput, calls=%fused_computation.399 | convolution fusion | flops 536870912 | bytes 3670016 | tf_op jit(solution)/shard_map/dot_general | solution.py:49
  133.1 2.7 %fusion.219 = f32[512,256]{1,0:T(8,128)} fusion(bf16[512,2048]{1,0:T(8,128)(2,1)S(1)} %bitcast.201, bf16[2048,256]{1,0:T(8,128)(2,1)} %collective-permute-done.19), kind=kOutput, calls=%fused_computation.401 | convolution fusion | flops 536870912 | bytes 3670016 | tf_op jit(solution)/shard_map/dot_general | solution.py:49
  135.8 6.0 %fusion.16 = f32[512,2048]{1,0:T(8,128)} fusion(bf16[256,2048]{1,0:T(8,128)(2,1)} %collective-permute-done.18, f32[512,256]{1,0:T(8,128)} %fusion.218, bf16[512,2048]{1,0:T(8,128)(2,1)S(1)} %bitcast.202, bf16[2048,256]{1,0:T(8,128)(2,1)} %collective-permute-done.17), kind=kOutput, calls=%fused_computation.35 | convolution fusion | flops 1074528256 | bytes 8912896 | tf_op jit(solution)/shard_map/dot_general | solution.py:49
  141.8 6.0 %fusion.15 = f32[512,2048]{1,0:T(8,128)} fusion(bf16[256,2048]{1,0:T(8,128)(2,1)} %collective-permute-done.15, f32[512,256]{1,0:T(8,128)} %fusion.217, bf16[512,2048]{1,0:T(8,128)(2,1)S(1)} %bitcast.203, bf16[2048,256]{1,0:T(8,128)(2,1)} %collective-permute-done.14), kind=kOutput, calls=%fused_computation.34 | convolution fusion | flops 1074528256 | bytes 8912896 | tf_op jit(solution)/shard_map/dot_general | solution.py:49
  147.9 9.1 %add_convert_fusion = bf16[512,2048]{1,0:T(8,128)(2,1)} fusion(f32[512,2048]{1,0:T(8,128)} %fusion.16, f32[512,2048]{1,0:T(8,128)} %fusion.7, f32[512,2048]{1,0:T(8,128)} %fusion.15, bf16[256,2048]{1,0:T(8,128)(2,1)} %collective-permute-done.21, f32[512,256]{1,0:T(8,128)} %fusion.219, bf16[512,2048]{1,0:T(8,128)(2,1)S(1)} %bitcast.204, ...), kind=kOutput, calls=%fused_computation | convolution fusion | flops 1078722560 | bytes 19398656 | tf_op jit(solution)/shard_map/dot_general | solution.py:49
  156.9 5.7 %all-to-all-start.1 = ((bf16[8,64,2048]{2,1,0:T(8,128)(2,1)}), bf16[8,64,2048]{2,1,0:T(8,128)(2,1)S(1)}, u32[]{:S(2)}, u32[]{:S(2)}) async-start(bf16[8,64,2048]{2,1,0:T(8,128)(2,1)} %bitcast.207), calls=%async_computation.1 | async-start | bytes 4194304 | tf_op jit(solution)/shard_map/all_to_all | solution.py:154
  162.6 0.8 divide_multiply_fusion
  163.4 48.1 %all-to-all-done.1 = bf16[8,64,2048]{2,1,0:T(8,128)(2,1)S(1)} async-done(((bf16[8,64,2048]{2,1,0:T(8,128)(2,1)}), bf16[8,64,2048]{2,1,0:T(8,128)(2,1)S(1)}, u32[]{:S(2)}, u32[]{:S(2)}) %all-to-all-start.1) | async-done | bytes 2097184 | tf_op jit(solution)/shard_map/all_to_all | solution.py:154
  212.1 0.6 fusion.5
  212.7 0.8 copy-done.1
  213.6 1.0 collective-permute-start.23
  214.6 0.9 collective-permute-start.24
  215.4 3.9 %collective-permute-done.22 = bf16[128,512]{1,0:T(8,128)(2,1)S(1)} collective-permute-done((bf16[128,512]{1,0:T(8,128)(2,1)S(1)}, bf16[128,512]{1,0:T(8,128)(2,1)S(1)}, u32[]{:S(2)}, u32[]{:S(2)}) %collective-permute-start.22) | collective-permute-done | bytes 131104 | tf_op jit(solution)/shard_map/ppermute | solution.py:16
  219.4 1.9 collective-permute-done.23
  221.3 1.1 select_select_fusion.3
  222.3 0.8 pad_maximum_fusion
  (71 shorter events, 4.6 us)
Async XLA Ops:
  0.0 11.7 %copy-start = (s32[512,2]{0,1:T(2,128)S(1)}, s32[512,2]{0,1:T(2,128)}, u32[]{:S(2)}) copy-start(s32[512,2]{0,1:T(2,128)} %param.22) | copy-start | bytes 12292
  1.5 13.9 %collective-permute-start.4 = (f32[35,256]{1,0:T(8,128)S(1)}, f32[35,256]{1,0:T(8,128)S(1)}, u32[]{:S(2)}, u32[]{:S(2)}) collective-permute-start(f32[35,256]{1,0:T(8,128)S(1)} %pad_maximum_fusion.1), channel_id=1, source_target_pairs={{0,1},{1,0},{2,3},{3,2},{4,5},{5,4},{6,7},{7,6},{8,9},{9,8},{10,11... | collective-permute-start | bytes 107528 | tf_op jit(solution)/shard_map/ppermute | solution.py:16
  2.1 13.7 %collective-permute-start.6 = (f32[35,256]{1,0:T(8,128)S(1)}, f32[35,256]{1,0:T(8,128)S(1)}, u32[]{:S(2)}, u32[]{:S(2)}) collective-permute-start(f32[35,256]{1,0:T(8,128)S(1)} %pad_maximum_fusion.1), channel_id=1, source_target_pairs={{0,2},{1,3},{2,0},{3,1},{4,6},{5,7},{6,4},{7,5},{8,10},{9,11},{10,... | collective-permute-start | bytes 107528 | tf_op jit(solution)/shard_map/ppermute | solution.py:16
  4.7 11.4 %collective-permute-start.8 = (f32[35,256]{1,0:T(8,128)S(1)}, f32[35,256]{1,0:T(8,128)S(1)}, u32[]{:S(2)}, u32[]{:S(2)}) collective-permute-start(f32[35,256]{1,0:T(8,128)S(1)} %pad_maximum_fusion.1), channel_id=1, source_target_pairs={{0,3},{1,2},{2,1},{3,0},{4,7},{5,6},{6,5},{7,4},{8,11},{9,10},{10,... | collective-permute-start | bytes 107528 | tf_op jit(solution)/shard_map/ppermute | solution.py:16
  5.9 7.2 %collective-permute-start.3 = (bf16[32,256]{1,0:T(8,128)(2,1)S(1)}, bf16[32,256]{1,0:T(8,128)(2,1)S(1)}, u32[]{:S(2)}, u32[]{:S(2)}) collective-permute-start(bf16[32,256]{1,0:T(8,128)(2,1)S(1)} %slice.1046), channel_id=1, source_target_pairs={{0,4},{4,8},{8,12},{12,16},{16,20},{20,24},{24,28},{1,5},{5,9},{9,... | collective-permute-start | bytes 49160 | tf_op jit(solution)/shard_map/ppermute | solution.py:82
  9.5 42.0 %collective-permute-start.10 = (bf16[256,2048]{1,0:T(8,128)(2,1)}, bf16[256,2048]{1,0:T(8,128)(2,1)S(1)}, u32[]{:S(2)}, u32[]{:S(2)}) collective-permute-start(bf16[256,2048]{1,0:T(8,128)(2,1)} %param.19), channel_id=1, source_target_pairs={{0,1},{1,0},{2,3},{3,2},{4,5},{5,4},{6,7},{7,6},{8,9},{9,8},{10,11... | collective-permute-start | bytes 3145736 | tf_op jit(solution)/shard_map/ppermute | solution.py:16
  13.1 36.3 %collective-permute-start.11 = (bf16[256,2048]{1,0:T(8,128)(2,1)}, bf16[256,2048]{1,0:T(8,128)(2,1)S(1)}, u32[]{:S(2)}, u32[]{:S(2)}) collective-permute-start(bf16[256,2048]{1,0:T(8,128)(2,1)} %param.19), channel_id=1, source_target_pairs={{0,2},{1,3},{2,0},{3,1},{4,6},{5,7},{6,4},{7,5},{8,10},{9,11},{10,... | collective-permute-start | bytes 3145736 | tf_op jit(solution)/shard_map/ppermute | solution.py:16
  15.4 35.0 %collective-permute-start = (bf16[128,512]{1,0:T(8,128)(2,1)S(1)}, bf16[128,512]{1,0:T(8,128)(2,1)S(1)}, u32[]{:S(2)}, u32[]{:S(2)}) collective-permute-start(bf16[128,512]{1,0:T(8,128)(2,1)S(1)} %get-tuple-element.34), channel_id=1, source_target_pairs={{0,3},{1,2},{2,1},{3,0},{4,7},{5,6},{6,5},{7,4},{8,11},{9,10},{10,... | collective-permute-start | bytes 393224 | tf_op jit(solution)/shard_map/ppermute | solution.py:16
  15.7 2.1 collective-permute-start.5
  16.1 27.9 %collective-permute-start.7 = (bf16[160,256]{1,0:T(8,128)(2,1)S(1)}, bf16[160,256]{1,0:T(8,128)(2,1)S(1)}, u32[]{:S(2)}, u32[]{:S(2)}) collective-permute-start(bf16[160,256]{1,0:T(8,128)(2,1)S(1)} %get-tuple-element.37), channel_id=1, source_target_pairs={{0,2},{1,3},{2,0},{3,1},{4,6},{5,7},{6,4},{7,5},{8,10},{9,11},{10,... | collective-permute-start | bytes 245768 | tf_op jit(solution)/shard_map/ppermute | solution.py:16
  17.9 32.5 %collective-permute-start.1 = (bf16[128,512]{1,0:T(8,128)(2,1)S(1)}, bf16[128,512]{1,0:T(8,128)(2,1)S(1)}, u32[]{:S(2)}, u32[]{:S(2)}) collective-permute-start(bf16[128,512]{1,0:T(8,128)(2,1)S(1)} %get-tuple-element.33), channel_id=1, source_target_pairs={{0,2},{1,3},{2,0},{3,1},{4,6},{5,7},{6,4},{7,5},{8,10},{9,11},{10,... | collective-permute-start | bytes 393224 | tf_op jit(solution)/shard_map/ppermute | solution.py:16
  44.0 4.7 %collective-permute-start.9 = (bf16[160,256]{1,0:T(8,128)(2,1)S(1)}, bf16[160,256]{1,0:T(8,128)(2,1)S(1)}, u32[]{:S(2)}, u32[]{:S(2)}) collective-permute-start(bf16[160,256]{1,0:T(8,128)(2,1)S(1)} %get-tuple-element.38), channel_id=1, source_target_pairs={{0,3},{1,2},{2,1},{3,0},{4,7},{5,6},{6,5},{7,4},{8,11},{9,10},{10,... | collective-permute-start | bytes 245768 | tf_op jit(solution)/shard_map/ppermute | solution.py:16
  48.6 1.8 collective-permute-start.2
  48.8 1.2 copy-start.2
  48.8 1.2 copy-start.3
  48.8 1.2 copy-start.4
  49.4 2.9 %collective-permute-start.12 = (bf16[256,2048]{1,0:T(8,128)(2,1)S(1)}, bf16[256,2048]{1,0:T(8,128)(2,1)S(1)}, u32[]{:S(2)}, u32[]{:S(2)}) collective-permute-start(bf16[256,2048]{1,0:T(8,128)(2,1)S(1)} %collective-permute-done.11), channel_id=1, source_target_pairs={{0,1},{1,0},{2,3},{3,2},{4,5},{5,4},{6,7},{7,6},{8,9},{9,8},{10,11... | collective-permute-start | bytes 3145736 | tf_op jit(solution)/shard_map/ppermute | solution.py:16
  55.0 53.7 %all-to-all-start = ((bf16[8,64,2048]{2,1,0:T(8,128)(2,1)}), bf16[8,64,2048]{2,1,0:T(8,128)(2,1)S(1)}, u32[]{:S(2)}, u32[]{:S(2)}) async-start(bf16[8,64,2048]{2,1,0:T(8,128)(2,1)} %bitcast.208), calls=%async_computation | async-start | bytes 4194304 | tf_op jit(solution)/shard_map/all_to_all | solution.py:147
  59.9 26.3 %collective-permute-start.16 = (bf16[2048,256]{1,0:T(8,128)(2,1)}, bf16[2048,256]{1,0:T(8,128)(2,1)}, u32[]{:S(2)}, u32[]{:S(2)}) collective-permute-start(bf16[2048,256]{1,0:T(8,128)(2,1)} %bitcast.349), channel_id=1, source_target_pairs={{0,2},{1,3},{2,0},{3,1},{4,6},{5,7},{6,4},{7,5},{8,10},{9,11},{10,... | collective-permute-start | bytes 3145736 | tf_op jit(solution)/shard_map/ppermute | solution.py:16
  60.7 59.5 %collective-permute-start.13 = (bf16[2048,256]{1,0:T(8,128)(2,1)}, bf16[2048,256]{1,0:T(8,128)(2,1)}, u32[]{:S(2)}, u32[]{:S(2)}) collective-permute-start(bf16[2048,256]{1,0:T(8,128)(2,1)} %bitcast.350), channel_id=1, source_target_pairs={{0,1},{1,0},{2,3},{3,2},{4,5},{5,4},{6,7},{7,6},{8,9},{9,8},{10,11... | collective-permute-start | bytes 3145736 | tf_op jit(solution)/shard_map/ppermute | solution.py:16
  60.7 81.2 %collective-permute-start.14 = (bf16[2048,256]{1,0:T(8,128)(2,1)}, bf16[2048,256]{1,0:T(8,128)(2,1)}, u32[]{:S(2)}, u32[]{:S(2)}) collective-permute-start(bf16[2048,256]{1,0:T(8,128)(2,1)} %bitcast.209), channel_id=1, source_target_pairs={{0,1},{1,0},{2,3},{3,2},{4,5},{5,4},{6,7},{7,6},{8,9},{9,8},{10,11... | collective-permute-start | bytes 3145736 | tf_op jit(solution)/shard_map/ppermute | solution.py:16
  61.2 59.0 %collective-permute-start.17 = (bf16[2048,256]{1,0:T(8,128)(2,1)}, bf16[2048,256]{1,0:T(8,128)(2,1)}, u32[]{:S(2)}, u32[]{:S(2)}) collective-permute-start(bf16[2048,256]{1,0:T(8,128)(2,1)} %bitcast.210), channel_id=1, source_target_pairs={{0,2},{1,3},{2,0},{3,1},{4,6},{5,7},{6,4},{7,5},{8,10},{9,11},{10,... | collective-permute-start | bytes 3145736 | tf_op jit(solution)/shard_map/ppermute | solution.py:16
  62.4 67.9 %collective-permute-start.18 = (bf16[256,2048]{1,0:T(8,128)(2,1)}, bf16[256,2048]{1,0:T(8,128)(2,1)}, u32[]{:S(2)}, u32[]{:S(2)}) collective-permute-start(bf16[256,2048]{1,0:T(8,128)(2,1)} %bitcast.211), channel_id=1, source_target_pairs={{0,2},{1,3},{2,0},{3,1},{4,6},{5,7},{6,4},{7,5},{8,10},{9,11},{10,... | collective-permute-start | bytes 3145736 | tf_op jit(solution)/shard_map/ppermute | solution.py:16
  86.2 46.8 %collective-permute-start.19 = (bf16[2048,256]{1,0:T(8,128)(2,1)}, bf16[2048,256]{1,0:T(8,128)(2,1)}, u32[]{:S(2)}, u32[]{:S(2)}) collective-permute-start(bf16[2048,256]{1,0:T(8,128)(2,1)} %collective-permute-done.16), channel_id=1, source_target_pairs={{0,1},{1,0},{2,3},{3,2},{4,5},{5,4},{6,7},{7,6},{8,9},{9,8},{10,11... | collective-permute-start | bytes 3145736 | tf_op jit(solution)/shard_map/ppermute | solution.py:16
  120.1 21.7 %collective-permute-start.15 = (bf16[256,2048]{1,0:T(8,128)(2,1)}, bf16[256,2048]{1,0:T(8,128)(2,1)}, u32[]{:S(2)}, u32[]{:S(2)}) collective-permute-start(bf16[256,2048]{1,0:T(8,128)(2,1)} %bitcast.212), channel_id=1, source_target_pairs={{0,1},{1,0},{2,3},{3,2},{4,5},{5,4},{6,7},{7,6},{8,9},{9,8},{10,11... | collective-permute-start | bytes 3145736 | tf_op jit(solution)/shard_map/ppermute | solution.py:16
  120.1 27.7 %collective-permute-start.20 = (bf16[2048,256]{1,0:T(8,128)(2,1)}, bf16[2048,256]{1,0:T(8,128)(2,1)}, u32[]{:S(2)}, u32[]{:S(2)}) collective-permute-start(bf16[2048,256]{1,0:T(8,128)(2,1)} %collective-permute-done.17), channel_id=1, source_target_pairs={{0,1},{1,0},{2,3},{3,2},{4,5},{5,4},{6,7},{7,6},{8,9},{9,8},{10,11... | collective-permute-start | bytes 3145736 | tf_op jit(solution)/shard_map/ppermute | solution.py:16
  130.3 17.5 %collective-permute-start.21 = (bf16[256,2048]{1,0:T(8,128)(2,1)}, bf16[256,2048]{1,0:T(8,128)(2,1)}, u32[]{:S(2)}, u32[]{:S(2)}) collective-permute-start(bf16[256,2048]{1,0:T(8,128)(2,1)} %collective-permute-done.18), channel_id=1, source_target_pairs={{0,1},{1,0},{2,3},{3,2},{4,5},{5,4},{6,7},{7,6},{8,9},{9,8},{10,11... | collective-permute-start | bytes 3145736 | tf_op jit(solution)/shard_map/ppermute | solution.py:16
  156.9 54.6 %all-to-all-start.1 = ((bf16[8,64,2048]{2,1,0:T(8,128)(2,1)}), bf16[8,64,2048]{2,1,0:T(8,128)(2,1)S(1)}, u32[]{:S(2)}, u32[]{:S(2)}) async-start(bf16[8,64,2048]{2,1,0:T(8,128)(2,1)} %bitcast.207), calls=%async_computation.1 | async-start | bytes 4194304 | tf_op jit(solution)/shard_map/all_to_all | solution.py:154
  212.7 0.8 copy-start.1
  213.5 5.9 %collective-permute-start.22 = (bf16[128,512]{1,0:T(8,128)(2,1)S(1)}, bf16[128,512]{1,0:T(8,128)(2,1)S(1)}, u32[]{:S(2)}, u32[]{:S(2)}) collective-permute-start(bf16[128,512]{1,0:T(8,128)(2,1)S(1)} %get-tuple-element.31), channel_id=1, source_target_pairs={{0,3},{1,2},{2,1},{3,0},{4,7},{5,6},{6,5},{7,4},{8,11},{9,10},{10,... | collective-permute-start | bytes 393224 | tf_op jit(solution)/shard_map/ppermute | solution.py:16
  213.6 7.7 %collective-permute-start.23 = (bf16[128,512]{1,0:T(8,128)(2,1)S(1)}, bf16[128,512]{1,0:T(8,128)(2,1)S(1)}, u32[]{:S(2)}, u32[]{:S(2)}) collective-permute-start(bf16[128,512]{1,0:T(8,128)(2,1)S(1)} %get-tuple-element.30), channel_id=1, source_target_pairs={{0,2},{1,3},{2,0},{3,1},{4,6},{5,7},{6,4},{7,5},{8,10},{9,11},{10,... | collective-permute-start | bytes 393224 | tf_op jit(solution)/shard_map/ppermute | solution.py:16
  214.6 6.7 %collective-permute-start.24 = (bf16[128,512]{1,0:T(8,128)(2,1)S(1)}, bf16[128,512]{1,0:T(8,128)(2,1)S(1)}, u32[]{:S(2)}, u32[]{:S(2)}) collective-permute-start(bf16[128,512]{1,0:T(8,128)(2,1)S(1)} %get-tuple-element.29), channel_id=1, source_target_pairs={{0,1},{1,0},{2,3},{3,2},{4,5},{5,4},{6,7},{7,6},{8,9},{9,8},{10,11... | collective-permute-start | bytes 393224 | tf_op jit(solution)/shard_map/ppermute | solution.py:16
